TPU v7x, 512 devices: a 8x2x16 block of a 8x16x16 slice. The times are simulated.
512 devices in a mesh: grp: 2 (over y), sp: 16 (over z), tp: 16 (over x, core).
Axes of the slice: x: 8, y: 2, z: 16, core: 2. Of those that a mesh axis runs over, the one named last changes fastest.
The devices are a block of a 8x16x16 slice.
Arguments:
- target: bfloat16 [4096, 2048], P(('grp', 'sp', 'tp')), parts along dimension 0, may hold values from -60 to 60
- source: bfloat16 [32768, 2048], P(('grp', 'sp', 'tp')), parts along dimension 0, may hold values from -120 to 120
- w_query: bfloat16 [2, 2048, 2048], P(None, None, 'tp'), may hold values from -0.176776695 to 0.176776695
- w_key: bfloat16 [2, 2048, 2048], P(None, None, 'tp'), may hold values from -0.176776695 to 0.176776695
- w_value: bfloat16 [2, 2048, 2048], P(None, None, 'tp'), may hold values from -0.125 to 0.125
- w_out: bfloat16 [2, 2048, 2048], P(None, 'tp'), may hold values from -0.125 to 0.125
- gains: float32 [2, 2, 2048], replicated, may hold values from 0.1 to 1.9
Outputs:
- mixed: bfloat16 [4096, 2048], P(('grp', 'sp', 'tp')), parts along dimension 0
There are 2 independent parts, one for each index of `grp`. A program takes and returns all parts, laid end to end along the dimension named above; an argument that names none is the same for every part. Nothing has to cross between parts.
All inputs are finite; a program needn't handle non-finite values.
Results may differ from a plain program's by a relative error of at most 0.025.
Values may be sent and summed in bfloat16 or wider, within the bound.
No kernel may reach another device: no remote copies, remote signals or barrier semaphores. Data moves between devices by JAX's collectives and lax.ppermute only.
A program may use at most 128 MiB of HBM per device.

v0:
```python
import jax
import jax.numpy as jnp
from jax import lax
from jax.sharding import Mesh
from jax.sharding import PartitionSpec as P

HEAD = 128
TP = ("tp_0", "tp_1")
GRP_SP_TP = ("grp", "sp", "tp_0", "tp_1")
EPS = 1e-06


def in_order(parts, dim):
    dims = list(parts.shape[1:])
    dims[dim] *= parts.shape[0]
    return jnp.moveaxis(parts, 0, dim).reshape(dims)


def stacked_from(x, axes, order):
    parts = x
    for k in order:
        parts = lax.all_gather(parts, axes[k])
    done = order[::-1]
    back = [done.index(k) for k in range(len(axes))]
    parts = parts.transpose(*back, *range(len(axes), parts.ndim))
    return parts.reshape(-1, *x.shape)


def whole_of(x, axes, order, dim):
    return in_order(stacked_from(x, axes, order), dim)


def sent_together(arrays, axis, dim, along):
    both = jnp.concatenate(arrays, axis=along)
    result, at, gathered = (lax.all_gather(both, axis, axis=dim, tiled=True), 0, [])
    for a in arrays:
        gathered.append(lax.slice_in_dim(result, at, at + a.shape[along], axis=along))
        at += a.shape[along]
    return tuple(gathered)


def split_up(x, dim, peers):
    dims = x.shape
    parts = x.reshape(*dims[:dim], peers, dims[dim] // peers, *dims[dim + 1 :])
    return jnp.moveaxis(parts, dim, 0)


def sum_at_owner(x, axis, dim):
    peers = lax.axis_size(axis)
    parts = lax.all_to_all(split_up(x, dim, peers), axis, 0, 0, tiled=True)
    return jnp.sum(parts.astype(jnp.float32), axis=0)


def normalize(row_block, gain_row):
    return (
        row_block
        * lax.rsqrt(jnp.mean(row_block * row_block, axis=-1, keepdims=True) + EPS)
        * gain_row
    )


def split_heads(row_block):
    return row_block.reshape(row_block.shape[0], row_block.shape[1] // HEAD, HEAD)


def body(target, source, w_query, w_key, w_value, w_out, gains):
    local_width = w_query.shape[2]
    heads_here = local_width // HEAD
    score_scale = HEAD ** (-0.5)
    depth = w_query.shape[0]
    project_shard_part = lax.all_gather(source, TP, axis=0, tiled=True)
    layer_parts = [
        jnp.stack(
            [
                jnp.dot(project_shard_part, w_key[level], preferred_element_type=jnp.float32),
                jnp.dot(project_shard_part, w_value[level], preferred_element_type=jnp.float32),
            ]
        )
        for level in range(depth)
    ]
    projected_source = jnp.stack(layer_parts).astype(jnp.bfloat16)
    stream = target.astype(jnp.float32)
    for layer_index in range(depth):
        normed = normalize(stream, gains[layer_index, 0]).astype(jnp.bfloat16)
        query_weight = w_query[layer_index]
        queries = jnp.dot(
            whole_of(normed, ("tp_0", "tp_1"), (0, 1), 0),
            query_weight,
            preferred_element_type=jnp.float32,
        ).astype(jnp.bfloat16)
        row_count = queries.shape[0]
        keys_here = projected_source[layer_index, 0]
        values_here = projected_source[layer_index, 1]
        query_heads = split_heads(queries)
        shard_part = sent_together((keys_here, values_here), "sp", 0, 1)
        row_peak = jnp.full((heads_here, row_count), -1e30, jnp.float32)
        key_heads = split_heads(shard_part[0])
        value_heads = split_heads(shard_part[1])
        scores = (
            jnp.einsum("qhd,khd->hqk", query_heads, key_heads, preferred_element_type=jnp.float32)
            * score_scale
        )
        new_peak = jnp.maximum(row_peak, jnp.max(scores, axis=2))
        weights = jnp.exp(scores - new_peak[:, :, None])
        row_total = jnp.sum(weights, axis=2)
        summed = jnp.einsum(
            "hqk,khd->hqd",
            weights.astype(jnp.bfloat16),
            value_heads,
            preferred_element_type=jnp.float32,
        )
        row_peak, row_total, summed = (new_peak, row_total, summed)
        heads_out = summed / row_total[:, :, None]
        attended = (
            jnp.transpose(heads_out, (1, 0, 2)).reshape(row_count, local_width).astype(jnp.bfloat16)
        )
        out_weight = w_out[layer_index]
        projected = sum_at_owner(
            jnp.dot(attended, out_weight, preferred_element_type=jnp.float32).astype(jnp.bfloat16),
            TP,
            0,
        )
        stream = stream + normalize(projected, gains[layer_index, 1])
    return stream.astype(jnp.bfloat16)


def solution(mesh):
    split = Mesh(
        mesh.devices.reshape(mesh.shape["grp"], mesh.shape["sp"], 8, 2),
        ("grp", "sp", "tp_0", "tp_1"),
    )
    placed = (
        P(GRP_SP_TP, None),
        P(GRP_SP_TP, None),
        P(None, None, TP),
        P(None, None, TP),
        P(None, None, TP),
        P(None, TP, None),
        P(),
    )
    return jax.shard_map(
        body, mesh=split, in_specs=placed, out_specs=P(GRP_SP_TP, None), check_vma=False
    )
```

profile of v0, /device:TPU:65, one launch (start us, length us, event | category | flops | bytes accessed | tf_op | source)
XLA Modules:
  0.0 365.9 jit_solution(10650329462650321292)
XLA Ops:
  6.6 0.7 all-gather.8.cloned.1.call-update
  7.4 85.2 %all-gather.8.cloned.1.call-done = bf16[1024,2048]{1,0:T(8,128)(2,1)} async-done(((bf16[64,2048]{1,0:T(8,128)(2,1)}), bf16[1024,2048]{1,0:T(8,128)(2,1)}) %all-gather.8.cloned.1.call-update) | async-done | bytes 4194320 | tf_op jit(solution)/shard_map/all_gather | solution.py:71
  92.6 3.8 %fusion.16 = bf16[1,1024,128]{1,2,0:T(8,128)(2,1)S(1)} fusion(bf16[1024,2048]{1,0:T(8,128)(2,1)} %all-gather.8.cloned.1.call-done, bf16[2,2048,128]{2,1,0:T(8,128)(2,1)} %param.10), kind=kOutput, calls=%fused_computation.24 | convolution fusion | flops 537001984 | bytes 4980736 | tf_op jit(solution)/shard_map/dot_general | solution.py:75
  96.4 3.8 %fusion.17 = bf16[1,1024,128]{1,2,0:T(8,128)(2,1)S(1)} fusion(bf16[1024,2048]{1,0:T(8,128)(2,1)} %all-gather.8.cloned.1.call-done, bf16[2,2048,128]{2,1,0:T(8,128)(2,1)} %param.11), kind=kOutput, calls=%fused_computation.25 | convolution fusion | flops 537001984 | bytes 4980736 | tf_op jit(solution)/shard_map/dot_general | solution.py:76
  100.4 0.8 pad_maximum_fusion
  101.4 3.8 %fusion.18 = bf16[1,1024,128]{1,2,0:T(8,128)(2,1)S(1)} fusion(bf16[1024,2048]{1,0:T(8,128)(2,1)} %all-gather.8.cloned.1.call-done, bf16[2,2048,128]{2,1,0:T(8,128)(2,1)S(1)} %copy-done), kind=kOutput, calls=%fused_computation.26 | convolution fusion | flops 537001984 | bytes 4980736 | tf_op jit(solution)/shard_map/dot_general | solution.py:75
  105.2 3.7 %fusion.19 = bf16[1,1024,128]{1,2,0:T(8,128)(2,1)S(1)} fusion(bf16[1024,2048]{1,0:T(8,128)(2,1)} %all-gather.8.cloned.1.call-done, bf16[2,2048,128]{2,1,0:T(8,128)(2,1)S(1)} %copy-done.1), kind=kOutput, calls=%fused_computation.27 | convolution fusion | flops 537001984 | bytes 4980736 | tf_op jit(solution)/shard_map/dot_general | solution.py:76
  109.0 0.9 pad_maximum_fusion.1
  110.2 19.9 %all-gather = bf16[64,2048]{1,0:T(8,128)(2,1)S(1)} all-gather(bf16[8,2048]{1,0:T(8,128)(2,1)S(1)} %fusion.70), channel_id=2, replica_groups=mesh['grp'=2,'sp'=16,'tp_0'=8,'tp_1'=2] {'tp_0'}, dimensions={0}, use_global_device_ids=true | all-gather | bytes 294912 | tf_op jit(solution)/shard_map/all_gather | solution.py:22
  130.0 7.1 %all-gather.1 = bf16[16,8,2048]{2,1,0:T(8,128)(2,1)S(1)} all-gather(bf16[8,8,2048]{2,1,0:T(8,128)(2,1)S(1)} %bitcast.78), channel_id=3, replica_groups=mesh['grp'=2,'sp'=16,'tp_0'=8,'tp_1'=2] {'tp_1'}, dimensions={0}, use_global_device_ids=true | all-gather | bytes 786432 | tf_op jit(solution)/shard_map/all_gather | solution.py:22
  137.1 71.2 %all-gather.10.cloned.1.call-done = bf16[16384,256]{0,1:T(8,128)(2,1)} async-done(((bf16[1024,256]{0,1:T(8,128)(2,1)}), bf16[16384,256]{0,1:T(8,128)(2,1)}) %all-gather.10.cloned.1.call-update) | async-done | bytes 8388624 | tf_op jit(solution)/shard_map/all_gather | solution.py:35
  208.4 7.0 %fusion.74 = (f32[128]{0:T(128)S(1)}, f32[128,16384]{1,0:T(8,128)}) fusion(bf16[16384,256]{0,1:T(8,128)(2,1)} %all-gather.10.cloned.1.call-done, bf16[128,2048]{1,0:T(8,128)(2,1)S(1)} %bitcast.76, bf16[2,2048,128]{2,1,0:T(8,128)(2,1)S(1)} %copy-done.3), kind=kOutput, calls=%fused_computation.80 | convolution fusion | flops 608190336 | bytes 13632000 | tf_op jit(solution)/shard_map/qhd,khd->hqk/dot_general | solution.py:100
  215.3 4.7 %fusion = f32[128]{0:T(128)S(1)} fusion(f32[128,16384]{1,0:T(8,128)} %get-tuple-element.14, f32[128]{0:T(128)S(1)} %broadcast_maximum_fusion.1), kind=kLoop, calls=%fused_computation.4 | loop fusion | flops 4194176 | bytes 8389632 | tf_op jit(solution)/shard_map/reduce_sum | solution.py:105
  220.0 6.4 %fusion.14 = bf16[16,8,2048]{2,1,0:T(8,128)(2,1)S(1)} fusion(bf16[16384,256]{0,1:T(8,128)(2,1)} %all-gather.10.cloned.1.call-done, f32[128,16384]{1,0:T(8,128)} %get-tuple-element.14, f32[128]{0:T(128)S(1)} %broadcast_maximum_fusion.1, bf16[2,128,2048]{2,1,0:T(8,128)(2,1)S(1)} %copy-done.2, f32[128]{0:T(128)S(1)} %fusion), kind=kOutput, calls=%fused_computation.18 | convolution fusion | flops 608468992 | bytes 13632512 | tf_op jit(solution)/shard_map/dot_general | solution.py:119
  226.4 24.5 %all_to_all.10 = bf16[16,8,2048]{2,1,0:T(8,128)(2,1)S(1)} all-to-all(bf16[16,8,2048]{2,1,0:T(8,128)(2,1)S(1)} %fusion.14), channel_id=1, replica_groups=mesh['grp'=2,'sp'=16,'tp_0'=8,'tp_1'=2] {'tp_0','tp_1'}, dimensions={0} | all-to-all | bytes 1048576 | tf_op jit(solution)/shard_map/all_to_all | solution.py:50
  251.2 0.2 multiply_reduce_fusion.1
  251.5 21.5 %all-gather.2 = bf16[64,2048]{1,0:T(8,128)(2,1)S(1)} all-gather(bf16[8,2048]{1,0:T(8,128)(2,1)S(1)} %multiply_convert_fusion), channel_id=4, replica_groups=mesh['grp'=2,'sp'=16,'tp_0'=8,'tp_1'=2] {'tp_0'}, dimensions={0}, use_global_device_ids=true | all-gather | bytes 294912 | tf_op jit(solution)/shard_map/all_gather | solution.py:22
  272.9 4.2 %all-gather.3 = bf16[16,8,2048]{2,1,0:T(8,128)(2,1)S(1)} all-gather(bf16[8,8,2048]{2,1,0:T(8,128)(2,1)S(1)} %bitcast.79), channel_id=5, replica_groups=mesh['grp'=2,'sp'=16,'tp_0'=8,'tp_1'=2] {'tp_1'}, dimensions={0}, use_global_device_ids=true | all-gather | bytes 786432 | tf_op jit(solution)/shard_map/all_gather | solution.py:22
  277.2 38.7 %all-gather.12.cloned.1.call-done = bf16[16384,256]{0,1:T(8,128)(2,1)} async-done(((bf16[1024,256]{0,1:T(8,128)(2,1)}), bf16[16384,256]{0,1:T(8,128)(2,1)}) %all-gather.12.cloned.1.call-update) | async-done | bytes 8388624 | tf_op jit(solution)/shard_map/all_gather | solution.py:35
  315.9 6.9 %fusion.77 = (f32[128]{0:T(128)S(1)}, f32[128,16384]{1,0:T(8,128)}) fusion(bf16[16384,256]{0,1:T(8,128)(2,1)} %all-gather.12.cloned.1.call-done, bf16[128,2048]{1,0:T(8,128)(2,1)S(1)} %bitcast.77, bf16[2,2048,128]{2,1,0:T(8,128)(2,1)S(1)} %copy-done.3), kind=kOutput, calls=%fused_computation.81 | convolution fusion | flops 608190336 | bytes 13632000 | tf_op jit(solution)/shard_map/qhd,khd->hqk/dot_general | solution.py:100
  322.8 4.7 %fusion.2 = f32[128]{0:T(128)S(1)} fusion(f32[128,16384]{1,0:T(8,128)} %get-tuple-element.16, f32[128]{0:T(128)S(1)} %broadcast_maximum_fusion), kind=kLoop, calls=%fused_computation.6 | loop fusion | flops 4194176 | bytes 8389632 | tf_op jit(solution)/shard_map/reduce_sum | solution.py:105
  327.5 6.4 %fusion.15 = bf16[16,8,2048]{2,1,0:T(8,128)(2,1)S(1)} fusion(bf16[16384,256]{0,1:T(8,128)(2,1)} %all-gather.12.cloned.1.call-done, f32[128,16384]{1,0:T(8,128)} %get-tuple-element.16, f32[128]{0:T(128)S(1)} %broadcast_maximum_fusion, bf16[2,128,2048]{2,1,0:T(8,128)(2,1)S(1)} %copy-done.2, f32[128]{0:T(128)S(1)} %fusion.2), kind=kOutput, calls=%fused_computation.19 | convolution fusion | flops 608468992 | bytes 13632512 | tf_op jit(solution)/shard_map/dot_general | solution.py:119
  333.9 24.6 %all_to_all.11 = bf16[16,8,2048]{2,1,0:T(8,128)(2,1)S(1)} all-to-all(bf16[16,8,2048]{2,1,0:T(8,128)(2,1)S(1)} %fusion.15), channel_id=1, replica_groups=mesh['grp'=2,'sp'=16,'tp_0'=8,'tp_1'=2] {'tp_0','tp_1'}, dimensions={0} | all-to-all | bytes 1048576 | tf_op jit(solution)/shard_map/all_to_all | solution.py:50
  358.6 0.7 add_convert_fusion
  (37 shorter events, 1.3 us)
Async XLA Ops:
  6.5 94.8 %copy-start = (bf16[2,2048,128]{2,1,0:T(8,128)(2,1)S(1)}, bf16[2,2048,128]{2,1,0:T(8,128)(2,1)}, u32[]{:S(2)}) copy-start(bf16[2,2048,128]{2,1,0:T(8,128)(2,1)} %param.10) | copy-start | bytes 3145732
  6.5 86.1 %all-gather.8.cloned.1.call-start = ((), (), s32[]{:S(2)}) async-start(), calls=%async_computation.2 | async-start | bytes 4456448 | tf_op jit(solution)/shard_map/all_gather | solution.py:71
  7.3 97.8 %copy-start.1 = (bf16[2,2048,128]{2,1,0:T(8,128)(2,1)S(1)}, bf16[2,2048,128]{2,1,0:T(8,128)(2,1)}, u32[]{:S(2)}) copy-start(bf16[2,2048,128]{2,1,0:T(8,128)(2,1)} %param.11) | copy-start | bytes 3145732
  7.3 201.0 %all-gather.10.cloned.1.call-start = ((), (), s32[]{:S(2)}) async-start(), calls=%async_computation.3 | async-start | bytes 8912896 | tf_op jit(solution)/shard_map/all_gather | solution.py:35
  100.3 9.6 %copy-start.4 = (bf16[8,2048]{1,0:T(8,128)(2,1)S(1)}, bf16[8,2048]{1,0:T(8,128)(2,1)}, u32[]{:S(2)}) copy-start(bf16[8,2048]{1,0:T(8,128)(2,1)} %param.7) | copy-start | bytes 98308
  100.3 9.7 %copy-start.5 = (f32[2,2,2048]{2,1,0:T(2,128)S(1)}, f32[2,2,2048]{2,1,0:T(2,128)}, u32[]{:S(2)}) copy-start(f32[2,2,2048]{2,1,0:T(2,128)} %param.13) | copy-start | bytes 98308
  101.2 107.1 %copy-start.3 = (bf16[2,2048,128]{2,1,0:T(8,128)(2,1)S(1)}, bf16[2,2048,128]{2,1,0:T(8,128)(2,1)}, u32[]{:S(2)}) copy-start(bf16[2,2048,128]{2,1,0:T(8,128)(2,1)} %param.9) | copy-start | bytes 3145732
  101.3 214.7 %all-gather.12.cloned.1.call-start = ((), (), s32[]{:S(2)}) async-start(), calls=%async_computation.4 | async-start | bytes 8912896 | tf_op jit(solution)/shard_map/all_gather | solution.py:35
  208.4 11.7 %copy-start.2 = (bf16[2,128,2048]{2,1,0:T(8,128)(2,1)S(1)}, bf16[2,128,2048]{2,1,0:T(8,128)(2,1)}, u32[]{:S(2)}) copy-start(bf16[2,128,2048]{2,1,0:T(8,128)(2,1)} %param.12) | copy-start | bytes 3145732
Sparse Core Ops, SparseCore 0:
  9.5 83.0 all-gather.7
  101.4 106.9 all-gather.9
  210.5 105.4 all-gather.11
where the time goes:
time: 366 us
  waiting for transfers between devices  196 us (54%)
  blocking collectives  102 us (28%)
  matrix products  41.7 us (11%)
  between operations  13.3 us (4%)
  other arithmetic  12.8 us (3%)
    all_gather x2, waiting for transfers between devices, sent_together(): lax.all_gather(both, axis, axis=dim, tiled=True)  110 us
    all_gather x1, waiting for transfers between devices, body(): project_shard_part = lax.all_gather(source, TP, axis=0, tiled=True)  85.2 us
    all_gather x4, blocking collectives, stacked_from(): parts = lax.all_gather(parts, axes[k])  52.6 us
    all_to_all x2, blocking collectives, sum_at_owner(): parts = lax.all_to_all(split_up(x, dim, peers), axis, 0, 0, tiled=True)  49.1 us
    dot_general x2, matrix products, body(): jnp.einsum('qhd,khd->hqk', query_heads, key_heads, preferred_element_type...  13.9 us
    dot_general x2, matrix products, body(): jnp.dot(attended, out_weight, preferred_element_type=jnp.float32)  12.7 us
    reduce_sum x2, other arithmetic, body(): row_total = jnp.sum(weights, axis=2)  9.35 us
    dot_general x2, matrix products, body(): jnp.dot(project_shard_part, w_key[level], preferred_element_type=jnp.floa...  7.6 us
  transfers between devices with their start and end apart: 3, of which 3 were waited for; matrix products, arithmetic and copies ran while one was open for 7% of the time, Pallas kernels for 0%

commit v1 on v0

--- a/solution.py
+++ b/solution.py
@@ -68,7 +68,9 @@
     heads_here = local_width // HEAD
     score_scale = HEAD ** (-0.5)
     depth = w_query.shape[0]
-    project_shard_part = lax.all_gather(source, TP, axis=0, tiled=True)
+    project_shard_part = jnp.concatenate(
+        lax.all_to_all(jnp.stack([source] * lax.axis_size(TP)), TP, 0, 0), axis=0
+    )
     layer_parts = [
         jnp.stack(
             [

time: 366 us -> 413 us (1.13)
  blocking collectives: 102 us -> 240 us
  waiting for transfers between devices: 196 us -> 106 us
  matrix products: 41.7 us -> 37.1 us
    all_to_all x0 -> x1, blocking collectives: none -> 140 us  [body(): lax.all_to_all(jnp.stack([source] * lax.axis_size(TP)), TP, 0, 0)]
    all_gather x1 -> x0, waiting for transfers between devices: 85.2 us -> none  [body(): project_shard_part = lax.all_gather(source, TP, axis=0, tiled=True)]
  transfers between devices with their start and end apart: 3 -> 2, of which waited for: 3 -> 2; matrix products, arithmetic and copies ran while one was open for 7% -> 7% of each run, Pallas kernels for 0% -> 0%
where the time goes in v1:
time: 413 us; the launch traced here: 412 us
  blocking collectives  240 us (58%)
  waiting for transfers between devices  106 us (26%)
  matrix products  37.1 us (9%)
  between operations  13.6 us (3%)
  other arithmetic  12.8 us (3%)
    all_to_all x1, blocking collectives, body(): lax.all_to_all(jnp.stack([source] * lax.axis_size(TP)), TP, 0, 0)  140 us
    all_gather x2, waiting for transfers between devices, sent_together(): lax.all_gather(both, axis, axis=dim, tiled=True)  106 us
    all_gather x4, blocking collectives, stacked_from(): parts = lax.all_gather(parts, axes[k])  51.2 us
    all_to_all x2, blocking collectives, sum_at_owner(): parts = lax.all_to_all(split_up(x, dim, peers), axis, 0, 0, tiled=True)  49.1 us
    dot_general x2, matrix products, body(): jnp.einsum('qhd,khd->hqk', query_heads, key_heads, preferred_element_type...  13.9 us
    dot_general x2, matrix products, body(): jnp.dot(attended, out_weight, preferred_element_type=jnp.float32)  12.7 us
    reduce_sum x2, other arithmetic, body(): row_total = jnp.sum(weights, axis=2)  9.35 us
  transfers between devices with their start and end apart: 2, of which 2 were waited for; matrix products, arithmetic and copies ran while one was open for 7% of the time, Pallas kernels for 0%

profile of v1, /device:TPU:65, one launch (start us, length us, event | category | flops | bytes accessed | tf_op | source)
XLA Modules:
  0.0 412.2 jit_solution(8094688842044721145)
XLA Ops:
  6.6 1.6 stack.53
  8.2 139.8 %all_to_all.15 = bf16[16,64,2048]{2,1,0:T(8,128)(2,1)S(1)} all-to-all(bf16[16,64,2048]{2,1,0:T(8,128)(2,1)S(1)} %stack.53), channel_id=1, replica_groups=mesh['grp'=2,'sp'=16,'tp_0'=8,'tp_1'=2] {'tp_0','tp_1'}, dimensions={0} | all-to-all | bytes 8388608 | tf_op jit(solution)/shard_map/all_to_all | solution.py:72
  147.9 1.5 fusion.16
  149.5 0.4 copy-done
  149.9 1.5 fusion.17
  151.5 0.8 pad_maximum_fusion
  152.5 3.8 fusion.18
  156.3 3.7 fusion.19
  160.1 0.9 pad_maximum_fusion.1
  161.3 20.4 %all-gather = bf16[64,2048]{1,0:T(8,128)(2,1)S(1)} all-gather(bf16[8,2048]{1,0:T(8,128)(2,1)S(1)} %fusion.70), channel_id=2, replica_groups=mesh['grp'=2,'sp'=16,'tp_0'=8,'tp_1'=2] {'tp_0'}, dimensions={0}, use_global_device_ids=true | all-gather | bytes 294912 | tf_op jit(solution)/shard_map/all_gather | solution.py:22
  181.7 5.2 %all-gather.1 = bf16[16,8,2048]{2,1,0:T(8,128)(2,1)S(1)} all-gather(bf16[8,8,2048]{2,1,0:T(8,128)(2,1)S(1)} %bitcast.83), channel_id=3, replica_groups=mesh['grp'=2,'sp'=16,'tp_0'=8,'tp_1'=2] {'tp_1'}, dimensions={0}, use_global_device_ids=true | all-gather | bytes 786432 | tf_op jit(solution)/shard_map/all_gather | solution.py:22
  187.0 67.4 %all-gather.7.cloned.1.call-done = bf16[16384,256]{0,1:T(8,128)(2,1)} async-done(((bf16[1024,256]{0,1:T(8,128)(2,1)}), bf16[16384,256]{0,1:T(8,128)(2,1)}) %all-gather.7.cloned.1.call-update) | async-done | bytes 8388624 | tf_op jit(solution)/shard_map/all_gather | solution.py:35
  254.4 7.0 %fusion.74 = (f32[128]{0:T(128)S(1)}, f32[128,16384]{1,0:T(8,128)}) fusion(bf16[16384,256]{0,1:T(8,128)(2,1)} %all-gather.7.cloned.1.call-done, bf16[128,2048]{1,0:T(8,128)(2,1)S(1)} %bitcast.81, bf16[2,2048,128]{2,1,0:T(8,128)(2,1)S(1)} %copy-done.4), kind=kOutput, calls=%fused_computation.80 | convolution fusion | flops 608190336 | bytes 13632000 | tf_op jit(solution)/shard_map/qhd,khd->hqk/dot_general | solution.py:102
  261.4 4.7 %fusion = f32[128]{0:T(128)S(1)} fusion(f32[128,16384]{1,0:T(8,128)} %get-tuple-element.14, f32[128]{0:T(128)S(1)} %broadcast_maximum_fusion.1), kind=kLoop, calls=%fused_computation.4 | loop fusion | flops 4194176 | bytes 8389632 | tf_op jit(solution)/shard_map/reduce_sum | solution.py:107
  266.0 6.4 %fusion.14 = bf16[16,8,2048]{2,1,0:T(8,128)(2,1)S(1)} fusion(bf16[16384,256]{0,1:T(8,128)(2,1)} %all-gather.7.cloned.1.call-done, f32[128,16384]{1,0:T(8,128)} %get-tuple-element.14, f32[128]{0:T(128)S(1)} %broadcast_maximum_fusion.1, bf16[2,128,2048]{2,1,0:T(8,128)(2,1)S(1)} %copy-done.3, f32[128]{0:T(128)S(1)} %fusion), kind=kOutput, calls=%fused_computation.18 | convolution fusion | flops 608468992 | bytes 13632512 | tf_op jit(solution)/shard_map/dot_general | solution.py:121
  272.4 24.6 %all_to_all.16 = bf16[16,8,2048]{2,1,0:T(8,128)(2,1)S(1)} all-to-all(bf16[16,8,2048]{2,1,0:T(8,128)(2,1)S(1)} %fusion.14), channel_id=1, replica_groups=mesh['grp'=2,'sp'=16,'tp_0'=8,'tp_1'=2] {'tp_0','tp_1'}, dimensions={0} | all-to-all | bytes 1048576 | tf_op jit(solution)/shard_map/all_to_all | solution.py:50
  297.5 21.3 %all-gather.2 = bf16[64,2048]{1,0:T(8,128)(2,1)S(1)} all-gather(bf16[8,2048]{1,0:T(8,128)(2,1)S(1)} %multiply_convert_fusion), channel_id=4, replica_groups=mesh['grp'=2,'sp'=16,'tp_0'=8,'tp_1'=2] {'tp_0'}, dimensions={0}, use_global_device_ids=true | all-gather | bytes 294912 | tf_op jit(solution)/shard_map/all_gather | solution.py:22
  318.8 4.2 %all-gather.3 = bf16[16,8,2048]{2,1,0:T(8,128)(2,1)S(1)} all-gather(bf16[8,8,2048]{2,1,0:T(8,128)(2,1)S(1)} %bitcast.84), channel_id=5, replica_groups=mesh['grp'=2,'sp'=16,'tp_0'=8,'tp_1'=2] {'tp_1'}, dimensions={0}, use_global_device_ids=true | all-gather | bytes 786432 | tf_op jit(solution)/shard_map/all_gather | solution.py:22
  323.0 38.9 %all-gather.9.cloned.1.call-done = bf16[16384,256]{0,1:T(8,128)(2,1)} async-done(((bf16[1024,256]{0,1:T(8,128)(2,1)}), bf16[16384,256]{0,1:T(8,128)(2,1)}) %all-gather.9.cloned.1.call-update) | async-done | bytes 8388624 | tf_op jit(solution)/shard_map/all_gather | solution.py:35
  361.9 6.9 %fusion.77 = (f32[128]{0:T(128)S(1)}, f32[128,16384]{1,0:T(8,128)}) fusion(bf16[16384,256]{0,1:T(8,128)(2,1)} %all-gather.9.cloned.1.call-done, bf16[128,2048]{1,0:T(8,128)(2,1)S(1)} %bitcast.82, bf16[2,2048,128]{2,1,0:T(8,128)(2,1)S(1)} %copy-done.4), kind=kOutput, calls=%fused_computation.81 | convolution fusion | flops 608190336 | bytes 13632000 | tf_op jit(solution)/shard_map/qhd,khd->hqk/dot_general | solution.py:102
  368.8 4.7 %fusion.2 = f32[128]{0:T(128)S(1)} fusion(f32[128,16384]{1,0:T(8,128)} %get-tuple-element.16, f32[128]{0:T(128)S(1)} %broadcast_maximum_fusion), kind=kLoop, calls=%fused_computation.6 | loop fusion | flops 4194176 | bytes 8389632 | tf_op jit(solution)/shard_map/reduce_sum | solution.py:107
  373.5 6.4 %fusion.15 = bf16[16,8,2048]{2,1,0:T(8,128)(2,1)S(1)} fusion(bf16[16384,256]{0,1:T(8,128)(2,1)} %all-gather.9.cloned.1.call-done, f32[128,16384]{1,0:T(8,128)} %get-tuple-element.16, f32[128]{0:T(128)S(1)} %broadcast_maximum_fusion, bf16[2,128,2048]{2,1,0:T(8,128)(2,1)S(1)} %copy-done.3, f32[128]{0:T(128)S(1)} %fusion.2), kind=kOutput, calls=%fused_computation.19 | convolution fusion | flops 608468992 | bytes 13632512 | tf_op jit(solution)/shard_map/dot_general | solution.py:121
  379.9 24.6 %all_to_all.17 = bf16[16,8,2048]{2,1,0:T(8,128)(2,1)S(1)} all-to-all(bf16[16,8,2048]{2,1,0:T(8,128)(2,1)S(1)} %fusion.15), channel_id=1, replica_groups=mesh['grp'=2,'sp'=16,'tp_0'=8,'tp_1'=2] {'tp_0','tp_1'}, dimensions={0} | all-to-all | bytes 1048576 | tf_op jit(solution)/shard_map/all_to_all | solution.py:50
  404.6 0.7 add_convert_fusion
  (38 shorter events, 1.4 us)
Async XLA Ops:
  6.5 141.4 %copy-start.1 = (bf16[2,2048,128]{2,1,0:T(8,128)(2,1)S(1)}, bf16[2,2048,128]{2,1,0:T(8,128)(2,1)}, u32[]{:S(2)}) copy-start(bf16[2,2048,128]{2,1,0:T(8,128)(2,1)} %param.10) | copy-start | bytes 3145732
  6.5 143.3 %copy-start.2 = (bf16[2,2048,128]{2,1,0:T(8,128)(2,1)S(1)}, bf16[2,2048,128]{2,1,0:T(8,128)(2,1)}, u32[]{:S(2)}) copy-start(bf16[2,2048,128]{2,1,0:T(8,128)(2,1)} %param.11) | copy-start | bytes 3145732
  6.6 247.8 %all-gather.7.cloned.1.call-start = ((), (), s32[]{:S(2)}) async-start(), calls=%async_computation.3 | async-start | bytes 8912896 | tf_op jit(solution)/shard_map/all_gather | solution.py:35
  147.9 1.9 copy-start
  151.4 9.6 %copy-start.5 = (bf16[8,2048]{1,0:T(8,128)(2,1)S(1)}, bf16[8,2048]{1,0:T(8,128)(2,1)}, u32[]{:S(2)}) copy-start(bf16[8,2048]{1,0:T(8,128)(2,1)} %param.7) | copy-start | bytes 98308
  151.5 9.7 %copy-start.6 = (f32[2,2,2048]{2,1,0:T(2,128)S(1)}, f32[2,2,2048]{2,1,0:T(2,128)}, u32[]{:S(2)}) copy-start(f32[2,2,2048]{2,1,0:T(2,128)} %param.13) | copy-start | bytes 98308
  152.3 102.0 %copy-start.4 = (bf16[2,2048,128]{2,1,0:T(8,128)(2,1)S(1)}, bf16[2,2048,128]{2,1,0:T(8,128)(2,1)}, u32[]{:S(2)}) copy-start(bf16[2,2048,128]{2,1,0:T(8,128)(2,1)} %param.9) | copy-start | bytes 3145732
  152.4 209.5 %all-gather.9.cloned.1.call-start = ((), (), s32[]{:S(2)}) async-start(), calls=%async_computation.4 | async-start | bytes 8912896 | tf_op jit(solution)/shard_map/all_gather | solution.py:35
  254.4 11.7 %copy-start.3 = (bf16[2,128,2048]{2,1,0:T(8,128)(2,1)S(1)}, bf16[2,128,2048]{2,1,0:T(8,128)(2,1)}, u32[]{:S(2)}) copy-start(bf16[2,128,2048]{2,1,0:T(8,128)(2,1)} %param.12) | copy-start | bytes 3145732
Sparse Core Ops, SparseCore 0:
  152.5 101.7 all-gather.6
  256.5 105.4 all-gather.8
